TPU v7x, 32 devices: a whole 2x2x4 slice. The times are simulated.
32 devices in a mesh: ep: 8 (over z, x), tp: 4 (over y, core).
Axes of the slice: x: 2, y: 2, z: 4, core: 2. Of those that a mesh axis runs over, the one named last changes fastest.
Arguments:
- mixer_input: bfloat16 [1024, 2048], P('ep'), may hold values from -6 to 6
- mixer_gain: float32 [2048], replicated, may hold values from 0.1 to 1.9
- outer_weight: bfloat16 [2048, 1024], P(None, 'tp'), may hold values from -0.125 to 0.125
- inner_weight: bfloat16 [2048, 1024], P(None, 'tp'), may hold values from -0.125 to 0.125
- value_weight: bfloat16 [2048, 1024], P(None, 'tp'), may hold values from -0.125 to 0.125
- conv_kernel: bfloat16 [3, 1024], P(None, 'tp'), may hold values from -3 to 3
- group_gain: float32 [1024], P('tp'), may hold values from 0.1 to 1.9
- mixer_out_weight: bfloat16 [1024, 2048], P(None, 'tp'), may hold values from -0.1875 to 0.1875
- expert_input: bfloat16 [2048, 2048], P('ep'), may hold values from -6 to 6
- expert_gain: float32 [2048], replicated, may hold values from 0.1 to 1.9
- routes: int32 [2048, 2], P('ep'), may hold values from 0 to 7, all different within a row; in each aligned block of 256 rows (0 to 255, 256 to 511, ...) at most 128 rows name the same one
- route_weight: float32 [2048, 2], P('ep'), may hold values from 0.1 to 1
- expert_gate: bfloat16 [8, 2048, 3584], P('ep', None, 'tp'), may hold values from -0.125 to 0.125
- expert_up: bfloat16 [8, 2048, 3584], P('ep', None, 'tp'), may hold values from -0.125 to 0.125
- expert_down: bfloat16 [8, 3584, 2048], P('ep', None, 'tp'), may hold values from -0.09375 to 0.09375
Outputs:
- mixed_tokens: bfloat16 [1024, 2048], P('ep', 'tp')
- expert_tokens: bfloat16 [2048, 2048], P('ep', 'tp')
Inputs may be any that keep to these rules, and one draw needn't show every extreme that they name: `routes`: each row names 2 different experts. Within the rows of one index of ep no expert is named by more than 128 rows, a bound that some block reaches of them.
All inputs are finite; a program needn't handle non-finite values.
Results may differ from a plain program's by a relative error of at most 0.014.
Values may be sent and summed in bfloat16 or wider, within the bound.
A program may use at most 64 MiB of HBM per device.

v0:
```python
import functools

import jax
import jax.numpy as jnp
from jax import lax
from jax.experimental import pallas as pl
from jax.experimental.pallas import tpu as pltpu
from jax.sharding import PartitionSpec as P

GROUP = 64


EPS = 1e-06


def from_behind(block, axis, distance):
    devices = range(lax.axis_size(axis))
    route = [(i - distance, i) for i in devices if i - distance in devices]
    return lax.ppermute(block, axis, route)


def rms_scale(values, gain):
    floats = values.astype(jnp.float32)
    scale = lax.rsqrt(jnp.mean(floats * floats, axis=-1, keepdims=True) + EPS)
    return floats * scale * gain


F32 = jnp.float32
BF16 = jnp.bfloat16


def flip(index, offset, count):
    out = index
    bit = 1
    while bit < count:
        if offset & bit:
            out = out + bit - 2 * bit * ((index // bit) % 2)
        bit *= 2
    return out


def matmul(a, b):
    return jnp.dot(a, b, preferred_element_type=F32)


def send_order(n_ep):
    half = n_ep // 2
    return [1, *range(half, n_ep), *range(2, half)]


def schedule(n_ep):
    half = n_ep // 2
    early = [*range(half, half + half // 2)]
    late = [*range(half + half // 2, n_ep)]
    steps = [("pass_far", m) for m in early]
    steps += [("finish", 0), ("mix", 0)]
    steps += [("far", m) for m in early] + [("pass_far", m) for m in late] + [("finish", 1)]
    done = list(early)
    for m, other in zip(range(2, half), late):
        steps += [("near", m), ("finish", done.pop(0)), ("far", other), ("finish", done.pop(0))]
        done += [m, other]
    return steps + [("finish", m) for m in done]


def experts_kernel(
    n_ep,
    mix_ref,
    mix_gain_ref,
    kernel_ref,
    group_gain_ref,
    x_ref,
    gain_ref,
    routes_ref,
    weight_ref,
    outer_hbm,
    inner_hbm,
    value_hbm,
    mix_out_hbm,
    gate_hbm,
    up_hbm,
    down_hbm,
    mix_o_ref,
    o_ref,
    nb,
    xs,
    xb,
    wgu,
    wd,
    hb,
    rs,
    ret,
    whi,
    wlo,
    na,
    wmix,
    wmo,
    padded,
    outer,
    grouped,
    w_sem,
    s_sem,
    r_sem,
):
    ep = lax.axis_index("ep")
    tp = lax.axis_index("tp")
    y, core = tp // 2, tp % 2
    partner = {"tp": y * 2 + 1 - core}
    across = {"tp": (1 - y) * 2 + core}
    over_tp = (1 - y) * 2 + core
    half = n_ep // 2
    rows = x_ref.shape[0]
    cap = xb.shape[2]
    span = xb.shape[3]
    tiles, depth, pair = wgu.shape
    tile = pair // 2
    part = hb.shape[3]
    out_cols = wd.shape[1]

    barrier = pltpu.get_barrier_semaphore()
    peers = [{"ep": flip(ep, m, n_ep)} for m in range(1, n_ep)] + [partner, across]
    for peer in peers:
        pl.semaphore_signal(barrier, inc=1, device_id=peer, device_id_type=pl.DeviceIdType.MESH)

    fetches = []
    for j in range(tiles):
        cols = pl.ds(j * tile, tile)
        fetches.append(
            (
                pltpu.make_async_copy(
                    gate_hbm.at[0, :, cols], wgu.at[j, :, pl.ds(0, tile)], w_sem.at[2 * j]
                ),
                pltpu.make_async_copy(
                    up_hbm.at[0, :, cols], wgu.at[j, :, pl.ds(tile, tile)], w_sem.at[2 * j + 1]
                ),
            )
        )
    fetch_down = pltpu.make_async_copy(down_hbm.at[0], wd, w_sem.at[2 * tiles])
    fetch_mix = [
        pltpu.make_async_copy(src, wmix.at[i], w_sem.at[2 * tiles + 1 + i])
        for i, src in enumerate((outer_hbm, inner_hbm, value_hbm))
    ]
    fetch_mix_out = pltpu.make_async_copy(mix_out_hbm, wmo, w_sem.at[2 * tiles + 4])
    for a, b in fetches:
        a.start()
        b.start()
    for copy in fetch_mix:
        copy.start()
    fetch_down.start()
    fetch_mix_out.start()

    step_rows = 32

    def normalize(src, gain, dst):
        def norm(i, carry):
            at = pl.ds(pl.multiple_of(i * step_rows, step_rows), step_rows)
            v = src[at, :].astype(F32)
            scale = lax.rsqrt(jnp.mean(v * v, axis=-1, keepdims=True) + EPS)
            dst[at, :] = (v * scale * gain[...]).astype(BF16)
            return carry

        lax.fori_loop(0, src.shape[0] // step_rows, norm, 0)

    normalize(x_ref, gain_ref, nb)

    first = routes_ref[0:1, :]
    second = routes_ref[1:2, :]
    masks = []
    level = lax.broadcasted_iota(jnp.int32, (n_ep, rows), 0)
    stacked = jnp.zeros((n_ep, rows), F32)
    for m in range(n_ep):
        e = flip(ep, m, n_ep)
        mask = jnp.where((first == e) | (second == e), 1.0, 0.0)
        masks.append(mask)
        stacked = jnp.where(level == m, mask, stacked)
    upper = lax.broadcasted_iota(jnp.int32, (rows, rows), 0) < lax.broadcasted_iota(
        jnp.int32, (rows, rows), 1
    )
    ranks = matmul(stacked.astype(BF16), jnp.where(upper, 1.0, 0.0).astype(BF16))
    slots = lax.broadcasted_iota(jnp.int32, (cap, rows), 0).astype(F32)
    place = []
    for m in range(n_ep):
        place.append(jnp.where((slots == ranks[m : m + 1, :]) & (masks[m] > 0.5), 1.0, 0.0))

    def remote(src, dst, kind, m, device):
        return pltpu.make_async_remote_copy(
            src_ref=src,
            dst_ref=dst,
            send_sem=s_sem.at[kind, m],
            recv_sem=r_sem.at[kind, m],
            device_id=device,
            device_id_type=pl.DeviceIdType.MESH,
        )

    mine2 = pl.ds(core * 2, 2)
    from_source, to_partner, to_across, relay = [None] * n_ep, {}, {}, {}
    for m in range(1, n_ep):
        peer = {"ep": flip(ep, m, n_ep)}
        if m < half:
            from_source[m] = remote(xs.at[m], xb.at[m, mine2], 0, m, peer)
            to_partner[m] = remote(xb.at[m, mine2], xb.at[m, mine2], 1, m, partner)
        else:
            from_source[m] = remote(xs.at[m, 0], xb.at[m, tp], 0, m, peer)
            to_partner[m] = remote(xb.at[m, tp], xb.at[m, tp], 1, m, partner)
            to_across[m] = remote(xb.at[m, tp], xb.at[m, tp], 2, m, across)
            relay[m] = remote(xb.at[m, over_tp], xb.at[m, over_tp], 3, m, partner)
    hid_partner, hid_across, hid_relay, back = [], [], [], [None] * n_ep
    for m in range(n_ep):
        hid_partner.append(remote(hb.at[m, tp], hb.at[m, tp], 4, m, partner))
        hid_across.append(remote(hb.at[m, tp], hb.at[m, tp], 5, m, across))
        hid_relay.append(remote(hb.at[m, over_tp], hb.at[m, over_tp], 6, m, partner))
        if m:
            back[m] = remote(rs.at[m], ret.at[m], 7, m, {"ep": flip(ep, m, n_ep)})

    for m in send_order(n_ep):
        chosen = place[m].astype(BF16)
        if m < half:
            for k in range(2):
                at = pl.ds(pl.multiple_of((core * 2 + k) * span, span), span)
                xs[m, k] = matmul(chosen, nb[:, at]).astype(BF16)
        else:
            at = pl.ds(pl.multiple_of(tp * span, span), span)
            xs[m, 0] = matmul(chosen, nb[:, at]).astype(BF16)
        if m == send_order(n_ep)[0]:
            pl.semaphore_wait(barrier, len(peers))
        from_source[m].start()
    chosen = place[0].astype(BF16)
    for k in range(depth // span):
        xb[0, k] = matmul(chosen, nb[:, k * span : (k + 1) * span]).astype(BF16)

    def expand(m):
        def body(j, carry):
            if m == 0:
                pltpu.make_async_copy(
                    gate_hbm.at[0, :, pl.ds(0, tile)], wgu.at[j, :, pl.ds(0, tile)], w_sem.at[2 * j]
                ).wait()
                pltpu.make_async_copy(
                    up_hbm.at[0, :, pl.ds(0, tile)],
                    wgu.at[j, :, pl.ds(tile, tile)],
                    w_sem.at[2 * j + 1],
                ).wait()
            acc = matmul(xb[m, 0], wgu[j, 0:span, :])
            for k in range(1, depth // span):
                acc = acc + matmul(xb[m, k], wgu[j, k * span : (k + 1) * span, :])
            g, u = acc[:, :tile], acc[:, tile:]
            hidden = g / (1.0 + jnp.exp(-g)) * u
            hb[m, tp, :, pl.ds(pl.multiple_of(j * tile, tile), tile)] = hidden.astype(BF16)
            return carry

        lax.fori_loop(0, tiles, body, 0)
        hid_across[m].start()
        hid_partner[m].start()

    block = 256

    def contract(m):
        hid_partner[m].wait_recv()
        hid_relay[m].wait_recv()
        for n in range(out_cols // block):
            cols = slice(n * block, (n + 1) * block)
            acc = matmul(hb[m, 0], wd[0:part, cols])
            for k in range(1, hb.shape[1]):
                acc = acc + matmul(hb[m, k], wd[k * part : (k + 1) * part, cols])
            if m == 0:
                ret[0, :, cols] = acc.astype(BF16)
            else:
                rs[m, :, cols] = acc.astype(BF16)
        if m:
            back[m].start()

    def pass_hidden(m):
        hid_across[m].wait_recv()
        hid_relay[m].start()

    def pass_near(m):
        from_source[m].wait_recv()
        to_partner[m].start()

    def pass_far(m):
        from_source[m].wait_recv()
        to_across[m].start()
        to_partner[m].start()

    def pass_relay(m):
        to_across[m].wait_recv()
        relay[m].start()

    def ready(m):
        to_partner[m].wait_recv()
        if m >= half:
            relay[m].wait_recv()

    mix_rows, channels = outer.shape
    halo = padded.shape[0] - mix_rows
    ahead = {"ep": lax.rem(ep + 1, n_ep)}
    send_halo = remote(padded.at[pl.ds(mix_rows, halo)], padded.at[pl.ds(0, halo)], 8, 0, ahead)
    mix_partner = remote(grouped.at[tp], grouped.at[tp], 8, 1, partner)
    mix_across = remote(grouped.at[tp], grouped.at[tp], 8, 2, across)
    mix_relay = remote(grouped.at[over_tp], grouped.at[over_tp], 8, 3, partner)

    def mix_project():
        normalize(mix_ref, mix_gain_ref, na)
        for copy in fetch_mix:
            copy.wait()
        outer[...] = matmul(na[...], wmix[0]).astype(BF16)
        inner = matmul(na[...], wmix[1]).astype(BF16).astype(F32)
        padded[pl.ds(halo, mix_rows), :] = inner * matmul(na[...], wmix[2]).astype(BF16).astype(F32)
        send_halo.start()

    def mix_convolve():
        send_halo.wait_recv()
        taps = kernel_ref[...].astype(F32)
        row = lax.broadcasted_iota(jnp.int32, (mix_rows, channels), 0)
        row = row + jnp.where(ep == 0, 0, mix_rows)
        conv = taps[2:3, :] * padded[pl.ds(halo, mix_rows), :]
        for back_by in (1, 2):
            shifted = padded[pl.ds(halo - back_by, mix_rows), :]
            conv = conv + taps[2 - back_by : 3 - back_by, :] * jnp.where(
                row >= back_by, shifted, 0.0
            )
        gated = outer[...].astype(F32) * conv
        squares = gated * gated
        group = lax.broadcasted_iota(jnp.int32, (mix_rows, channels), 1) // GROUP
        scale = jnp.zeros_like(gated)
        for i in range(channels // GROUP):
            mean = jnp.sum(jnp.where(group == i, squares, 0.0), axis=-1, keepdims=True) / GROUP
            scale = jnp.where(group == i, lax.rsqrt(mean + EPS), scale)
        grouped[tp] = (gated * scale * group_gain_ref[...]).astype(BF16)
        mix_across.start()
        mix_partner.start()

    def mix_pass():
        mix_across.wait_recv()
        mix_relay.start()

    def mix_contract():
        fetch_mix_out.wait()
        mix_partner.wait_recv()
        mix_relay.wait_recv()
        acc = matmul(grouped[0], wmo[0:channels, :])
        for k in range(1, grouped.shape[0]):
            acc = acc + matmul(grouped[k], wmo[k * channels : (k + 1) * channels, :])
        mix_o_ref[...] = acc.astype(BF16)

    def build_weights():
        for m in range(n_ep):
            picked = jnp.where(first == flip(ep, m, n_ep), weight_ref[0:1, :], weight_ref[1:2, :])
            scaled = (place[m] * picked).T
            high = scaled.astype(BF16)
            whi[:, m * cap : (m + 1) * cap] = high
            wlo[:, m * cap : (m + 1) * cap] = (scaled - high.astype(F32)).astype(BF16)

    def near(m):
        pass_near(m)
        ready(m)
        expand(m)

    def far(m):
        pass_relay(m)
        ready(m)
        expand(m)

    def finish(m):
        pass_hidden(m)
        contract(m)

    steps = dict(
        near=near, far=far, finish=finish, pass_far=pass_far, pass_hidden=pass_hidden,
        contract=contract,
    )
    expand(0)
    mix_project()
    build_weights()
    near(1)
    mix_convolve()
    fetch_down.wait()
    for step, m in schedule(n_ep):
        if step == "mix":
            mix_pass()
            mix_contract()
        else:
            steps[step](m)

    total = None
    for m in range(n_ep):
        if m:
            back[m].wait_recv()
        high = matmul(whi[:, m * cap : (m + 1) * cap], ret[m])
        low = matmul(wlo[:, m * cap : (m + 1) * cap], ret[m])
        total = high + low if total is None else total + (high + low)
    o_ref[...] = total.astype(BF16)

    for copy in (send_halo, mix_partner, mix_across, mix_relay):
        copy.wait_send()
    for m in range(n_ep):
        for copy in (hid_partner[m], hid_across[m], hid_relay[m], from_source[m], back[m]):
            if copy is not None:
                copy.wait_send()
        for table in (to_partner, to_across, relay):
            if m in table:
                table[m].wait_send()


def fused(
    mixer_input,
    mixer_gain,
    outer_weight,
    inner_weight,
    value_weight,
    conv_kernel,
    group_gain,
    mixer_out_weight,
    expert_input,
    expert_gain,
    routes,
    route_weight,
    expert_gate,
    expert_up,
    expert_down,
):
    n_ep, n_tp = lax.axis_size("ep"), lax.axis_size("tp")
    rows, width = expert_input.shape
    mix_rows = mixer_input.shape[0]
    channels = outer_weight.shape[1]
    cap = 2 * routes.shape[1] * rows // n_ep
    span = width // n_tp
    part = expert_gate.shape[2]
    tile = 128
    tiles = part // tile
    full, out_cols = expert_down.shape[1:]
    mix_cols = mixer_out_weight.shape[1]
    vmem = pl.BlockSpec(memory_space=pltpu.VMEM)
    hbm = pl.BlockSpec(memory_space=pl.ANY)
    return pl.pallas_call(
        functools.partial(experts_kernel, n_ep),
        out_shape=(
            jax.ShapeDtypeStruct((mix_rows, mix_cols), BF16),
            jax.ShapeDtypeStruct((rows, out_cols), BF16),
        ),
        in_specs=[vmem] * 8 + [hbm] * 7,
        out_specs=(vmem, vmem),
        scratch_shapes=[
            pltpu.VMEM((rows, width), BF16),
            pltpu.VMEM((n_ep, 2, cap, span), BF16),
            pltpu.VMEM((n_ep, n_tp, cap, span), BF16),
            pltpu.VMEM((tiles, width, 2 * tile), BF16),
            pltpu.VMEM((full, out_cols), BF16),
            pltpu.VMEM((n_ep, n_tp, cap, part), BF16),
            pltpu.VMEM((n_ep, cap, out_cols), BF16),
            pltpu.VMEM((n_ep, cap, out_cols), BF16),
            pltpu.VMEM((rows, n_ep * cap), BF16),
            pltpu.VMEM((rows, n_ep * cap), BF16),
            pltpu.VMEM((mix_rows, width), BF16),
            pltpu.VMEM((3, width, channels), BF16),
            pltpu.VMEM((channels * n_tp, mix_cols), BF16),
            pltpu.VMEM((8 + mix_rows, channels), F32),
            pltpu.VMEM((mix_rows, channels), BF16),
            pltpu.VMEM((n_tp, mix_rows, channels), BF16),
            pltpu.SemaphoreType.DMA((2 * tiles + 5,)),
            pltpu.SemaphoreType.DMA((9, n_ep)),
            pltpu.SemaphoreType.DMA((9, n_ep)),
        ],
        compiler_params=pltpu.CompilerParams(
            collective_id=0, has_side_effects=True, vmem_limit_bytes=60 * 1024 * 1024
        ),
        name="layer",
    )(
        mixer_input,
        mixer_gain.reshape(1, -1),
        conv_kernel,
        group_gain.reshape(1, -1),
        expert_input,
        expert_gain.reshape(1, -1),
        routes.T,
        route_weight.T,
        outer_weight,
        inner_weight,
        value_weight,
        mixer_out_weight,
        expert_gate,
        expert_up,
        expert_down,
    )


def fits(n_ep, n_tp, routes, expert_gate):
    return (
        n_tp == 4
        and n_ep >= 4
        and n_ep & (n_ep - 1) == 0
        and routes.shape[1] == 2
        and expert_gate.shape[0] == 1
        and expert_gate.shape[2] % 128 == 0
    )


def mixer_xla(
    mixer_input,
    mixer_gain,
    outer_weight,
    inner_weight,
    value_weight,
    conv_kernel,
    group_gain,
    mixer_out_weight,
):
    mix_count = mixer_input.shape[0]
    normed_a = rms_scale(mixer_input, mixer_gain).astype(jnp.bfloat16)
    outer = jnp.dot(normed_a, outer_weight, preferred_element_type=jnp.float32).astype(jnp.bfloat16)
    inner = jnp.dot(normed_a, inner_weight, preferred_element_type=jnp.float32).astype(jnp.bfloat16)
    values = jnp.dot(normed_a, value_weight, preferred_element_type=jnp.float32).astype(
        jnp.bfloat16
    )
    product = inner.astype(jnp.float32) * values.astype(jnp.float32)
    earlier_rows = from_behind(product[mix_count - 2 :], "ep", 1)
    padded = jnp.concatenate([earlier_rows, product], axis=0)
    kernel = conv_kernel.astype(jnp.float32)
    conv_sum = (
        kernel[0] * padded[0:mix_count]
        + kernel[1] * padded[1 : mix_count + 1]
        + kernel[2] * padded[2 : mix_count + 2]
    )
    gated = outer.astype(jnp.float32) * conv_sum
    grouped = gated.reshape(mix_count, -1, GROUP)
    grouped = rms_scale(grouped, group_gain.reshape(-1, GROUP))
    grouped = grouped.reshape(mix_count, -1).astype(jnp.bfloat16)
    weight_rows = mixer_out_weight
    mixed_tokens = jnp.dot(
        lax.all_gather(grouped, "tp", axis=1, tiled=True),
        weight_rows,
        preferred_element_type=jnp.float32,
    ).astype(jnp.bfloat16)
    return mixed_tokens


def experts_xla(
    expert_input,
    expert_gain,
    routes,
    route_weight,
    expert_gate,
    expert_up,
    expert_down,
):
    exp_count, picks_each = routes.shape
    width = expert_input.shape[1]
    experts = expert_gate.shape[0] * lax.axis_size("ep")
    capacity = 2 * picks_each * exp_count // experts
    normed_b = rms_scale(expert_input, expert_gain).astype(jnp.bfloat16)
    picks = routes.reshape(-1)
    onehot = (picks[:, None] == jnp.arange(experts, dtype=jnp.int32)[None, :]).astype(jnp.int32)
    rank = jnp.sum((jnp.cumsum(onehot, axis=0) - onehot) * onehot, axis=1)
    slot = picks * capacity + rank
    token = jnp.arange(exp_count * picks_each, dtype=jnp.int32) // picks_each
    table = jnp.zeros((experts * capacity,), jnp.int32).at[slot].set(token + 1)
    valid = table > 0
    gathered_rows = jnp.take(normed_b, jnp.maximum(table - 1, 0), axis=0)
    buffer = jnp.where(valid[:, None], gathered_rows, 0).reshape(experts, capacity, width)
    gate_weight = expert_gate[0]
    up_weight = expert_up[0]
    down_weight = expert_down[0]
    out_cols = down_weight.shape[1]
    span = width // lax.axis_size("tp")
    outgoing = lax.dynamic_slice_in_dim(buffer, lax.axis_index("tp") * span, span, 2)
    received = lax.all_to_all(outgoing, "ep", split_axis=0, concat_axis=0, tiled=True)
    sources = received.shape[0]
    count = received.shape[1]
    piece = lax.all_gather(received, "tp", axis=2, tiled=True)
    span = piece.shape[2]
    flat_piece = piece.reshape(sources * count, span)
    gate = jnp.dot(flat_piece, gate_weight, preferred_element_type=jnp.float32)
    up_value = jnp.dot(flat_piece, up_weight, preferred_element_type=jnp.float32)
    hidden = (jax.nn.silu(gate) * up_value).astype(jnp.bfloat16)
    weight_rows = down_weight
    results = jnp.dot(
        lax.all_gather(hidden, "tp", axis=1, tiled=True),
        weight_rows,
        preferred_element_type=jnp.float32,
    ).astype(jnp.bfloat16)
    returned = lax.all_to_all(
        results.reshape(sources, count, out_cols), "ep", split_axis=0, concat_axis=0, tiled=True
    )
    flat_returned = returned.reshape(experts * capacity, out_cols)
    chosen = (
        jnp.take(flat_returned, slot, axis=0)
        .astype(jnp.float32)
        .reshape(exp_count, picks_each, out_cols)
    )
    weighted = jnp.sum(chosen * route_weight[..., None], axis=1)
    expert_tokens = weighted.astype(jnp.bfloat16)
    return expert_tokens


def per_device(*args):
    n_ep, n_tp = lax.axis_size("ep"), lax.axis_size("tp")
    if fits(n_ep, n_tp, args[10], args[12]):
        return fused(*args)
    return mixer_xla(*args[:8]), experts_xla(*args[8:])


def solution(mesh):
    placed = (
        P("ep", None),
        P(),
        P(None, "tp"),
        P(None, "tp"),
        P(None, "tp"),
        P(None, "tp"),
        P("tp"),
        P(None, "tp"),
        P("ep", None),
        P(),
        P("ep", None),
        P("ep", None),
        P("ep", None, "tp"),
        P("ep", None, "tp"),
        P("ep", None, "tp"),
    )
    return jax.shard_map(
        per_device,
        mesh=mesh,
        in_specs=placed,
        out_specs=(P("ep", "tp"), P("ep", "tp")),
        check_vma=False,
    )
```

profile of v0, /device:TPU:11, one launch (start us, length us, event | category | flops | bytes accessed | tf_op | source)
XLA Modules:
  0.0 93.3 jit_solution(14722387767765875128)
XLA Ops:
  0.6 89.4 %layer.1 = (bf16[128,512]{1,0:T(8,128)(2,1)}, bf16[256,512]{1,0:T(8,128)(2,1)}) custom-call(bf16[128,2048]{1,0:T(8,128)(2,1)} %mix_ref.1, f32[1,2048]{1,0:T(1,128)} %bitcast.5, bf16[3,256]{1,0:T(4,128)(2,1)} %kernel_ref.1, f32[1,256]{1,0:T(1,128)} %bitcast.9, bf16[256,2048]{1,0:T(8,128)(2,1)} %x_ref.1, f32[1,2048]{1,0:T(1,128)} %bitcast.6, ...), custom_call_target="tpu_custom_call" | custom-call | tf_op jit(solution)/shard_map/layer/pallas_call | solution.py:433
  90.0 1.6 %copy.19 = bf16[128,512]{1,0:T(8,128)(2,1)} copy(bf16[128,512]{1,0:T(8,128)(2,1)} %get-tuple-element.4) | data formatting | bytes 262144
  91.6 1.7 %copy.20 = bf16[256,512]{1,0:T(8,128)(2,1)} copy(bf16[256,512]{1,0:T(8,128)(2,1)} %get-tuple-element.5) | data formatting | bytes 524288
where the time goes:
time: 94.6 us; the launch traced here: 93.3 us
  Pallas kernels  89.4 us (95%)
  local copies, waits for them, and re-layouts  3.24 us (3%)
    pallas_call x1, Pallas kernels, fused(): pl.pallas_call(functools.partial(experts_kernel, n_ep), out_shape=(jax.Sh...  89.4 us
    unnamed x2, local copies, waits for them, and re-layouts  3.24 us

commit v1 on v0

--- a/solution.py
+++ b/solution.py
@@ -33,8 +33,7 @@
     out = index
     bit = 1
     while bit < count:
-        if offset & bit:
-            out = out + bit - 2 * bit * ((index // bit) % 2)
+        out = out + bit * ((offset // bit) % 2) * (1 - 2 * ((index // bit) % 2))
         bit *= 2
     return out
 
@@ -43,35 +42,72 @@
     return jnp.dot(a, b, preferred_element_type=F32)
 
 
+def doubled(n_ep):
+    return [*range(n_ep - 1, n_ep)]
+
+
 def send_order(n_ep):
     half = n_ep // 2
-    return [1, *range(half, n_ep), *range(2, half)]
+    quarter = half // 2
+    far = [half + i + j * quarter for i in range(quarter) for j in range(2)]
+    return [1, *far[:2]], far[2:], [*range(half - 1, 1, -1)]
+
+
+def turns(n_ep):
+    half = n_ep // 2
+    return [0, 1, *range(half, n_ep), *range(half - 1, 1, -1)]
 
 
 def schedule(n_ep):
     half = n_ep // 2
-    early = [*range(half, half + half // 2)]
-    late = [*range(half + half // 2, n_ep)]
-    steps = [("pass_far", m) for m in early]
-    steps += [("finish", 0), ("mix", 0)]
-    steps += [("far", m) for m in early] + [("pass_far", m) for m in late] + [("finish", 1)]
-    done = list(early)
-    for m, other in zip(range(2, half), late):
-        steps += [("near", m), ("finish", done.pop(0)), ("far", other), ("finish", done.pop(0))]
-        done += [m, other]
-    return steps + [("finish", m) for m in done]
+    far = [m for m in range(half, n_ep) if m not in doubled(n_ep)]
+    order = turns(n_ep)
+    steps, crossing = [], [("hidden", 0)]
+
+    def take(item):
+        while item in crossing:
+            steps.append(crossing.pop(0))
+
+    def send(name, m, item):
+        steps.append((name, m))
+        crossing.append((item, m))
+
+    def arrive(m):
+        steps.append(("near" if m < half else "both", m))
+
+    arrive(1)
+    send("pass_far", far[0], "far")
+    for k in range(1, n_ep):
+        m = order[k]
+        take(("far", m))
+        if 2 <= k <= len(far):
+            send("pass_far", far[k - 1], "far")
+        steps += [("ready", m)]
+        if k + 1 == n_ep:
+            steps += [("contract", order[k - 2])]
+        send("expand", m, "hidden")
+        if k + 1 < n_ep and order[k + 1] not in far:
+            arrive(order[k + 1])
+        if k == 5:
+            send("mix_convolve", 0, "mix")
+        if 2 <= k < n_ep - 1:
+            steps += [("contract", order[k - 2])]
+        take(("hidden", order[k - 1]))
+    steps += [("contract", order[-2]), ("gather", 0), ("gather", 1)]
+    steps += [("last", 0), ("last", 1)]
+    return steps + [("gather", m) for m in order[2:]]
 
 
 def experts_kernel(
     n_ep,
-    mix_ref,
-    mix_gain_ref,
-    kernel_ref,
-    group_gain_ref,
-    x_ref,
-    gain_ref,
-    routes_ref,
-    weight_ref,
+    mix_hbm,
+    mix_gain_hbm,
+    kernel_hbm,
+    group_gain_hbm,
+    x_hbm,
+    gain_hbm,
+    routes_hbm,
+    weight_hbm,
     outer_hbm,
     inner_hbm,
     value_hbm,
@@ -81,6 +117,14 @@
     down_hbm,
     mix_o_ref,
     o_ref,
+    mix_ref,
+    mix_gain_ref,
+    kernel_ref,
+    group_gain_ref,
+    x_ref,
+    gain_ref,
+    routes_ref,
+    weight_ref,
     nb,
     xs,
     xb,
@@ -91,12 +135,14 @@
     ret,
     whi,
     wlo,
+    total,
     na,
     wmix,
     wmo,
     padded,
     outer,
     grouped,
+    i_sem,
     w_sem,
     s_sem,
     r_sem,
@@ -108,6 +154,8 @@
     across = {"tp": (1 - y) * 2 + core}
     over_tp = (1 - y) * 2 + core
     half = n_ep // 2
+    quarter = half // 2
+    inner = (ep // half + ep // quarter) % 2
     rows = x_ref.shape[0]
     cap = xb.shape[2]
     span = xb.shape[3]
@@ -121,6 +169,28 @@
     for peer in peers:
         pl.semaphore_signal(barrier, inc=1, device_id=peer, device_id_type=pl.DeviceIdType.MESH)
 
+    chunk = 64
+    chunks = rows // chunk
+    fetch_x = [
+        pltpu.make_async_copy(
+            x_hbm.at[pl.ds(i * chunk, chunk)], x_ref.at[pl.ds(i * chunk, chunk)], i_sem.at[i]
+        )
+        for i in range(chunks)
+    ]
+    fetch_small = [
+        pltpu.make_async_copy(src, dst, i_sem.at[chunks + i])
+        for i, (src, dst) in enumerate(
+            (
+                (gain_hbm, gain_ref),
+                (routes_hbm, routes_ref),
+                (weight_hbm, weight_ref),
+                (mix_gain_hbm, mix_gain_ref),
+                (kernel_hbm, kernel_ref),
+                (group_gain_hbm, group_gain_ref),
+                (mix_hbm, mix_ref),
+            )
+        )
+    ]
     fetches = []
     for j in range(tiles):
         cols = pl.ds(j * tile, tile)
@@ -140,17 +210,18 @@
         for i, src in enumerate((outer_hbm, inner_hbm, value_hbm))
     ]
     fetch_mix_out = pltpu.make_async_copy(mix_out_hbm, wmo, w_sem.at[2 * tiles + 4])
+    fetch_small[0].start()
+    for copy in fetch_x:
+        copy.start()
+    for copy in fetch_small[1:-1]:
+        copy.start()
     for a, b in fetches:
         a.start()
         b.start()
-    for copy in fetch_mix:
-        copy.start()
-    fetch_down.start()
-    fetch_mix_out.start()
 
     step_rows = 32
 
-    def normalize(src, gain, dst):
+    def normalize(src, gain, dst, start, count):
         def norm(i, carry):
             at = pl.ds(pl.multiple_of(i * step_rows, step_rows), step_rows)
             v = src[at, :].astype(F32)
@@ -158,10 +229,19 @@
             dst[at, :] = (v * scale * gain[...]).astype(BF16)
             return carry
 
-        lax.fori_loop(0, src.shape[0] // step_rows, norm, 0)
-
-    normalize(x_ref, gain_ref, nb)
-
+        lax.fori_loop(start // step_rows, (start + count) // step_rows, norm, 0)
+
+    fetch_small[0].wait()
+    for i in range(chunks):
+        fetch_x[i].wait()
+        normalize(x_ref, gain_ref, nb, i * chunk, chunk)
+    fetch_small[-1].start()
+    for copy in fetch_mix:
+        copy.start()
+    fetch_down.start()
+    fetch_mix_out.start()
+
+    fetch_small[1].wait()
     first = routes_ref[0:1, :]
     second = routes_ref[1:2, :]
     masks = []
@@ -177,9 +257,9 @@
     )
     ranks = matmul(stacked.astype(BF16), jnp.where(upper, 1.0, 0.0).astype(BF16))
     slots = lax.broadcasted_iota(jnp.int32, (cap, rows), 0).astype(F32)
-    place = []
-    for m in range(n_ep):
-        place.append(jnp.where((slots == ranks[m : m + 1, :]) & (masks[m] > 0.5), 1.0, 0.0))
+
+    def place(m):
+        return jnp.where((slots == ranks[m : m + 1, :]) & (masks[m] > 0.5), 1.0, 0.0)
 
     def remote(src, dst, kind, m, device):
         return pltpu.make_async_remote_copy(
@@ -191,28 +271,71 @@
             device_id_type=pl.DeviceIdType.MESH,
         )
 
+    def label(turn):
+        if turn < half:
+            return turn
+        r = turn - half
+        return turn + (1 - inner) * (quarter - 2 * quarter * (r // quarter))
+
+    def source_of(m):
+        return {"ep": flip(ep, m, n_ep)}
+
     mine2 = pl.ds(core * 2, 2)
-    from_source, to_partner, to_across, relay = [None] * n_ep, {}, {}, {}
-    for m in range(1, n_ep):
-        peer = {"ep": flip(ep, m, n_ep)}
-        if m < half:
-            from_source[m] = remote(xs.at[m], xb.at[m, mine2], 0, m, peer)
-            to_partner[m] = remote(xb.at[m, mine2], xb.at[m, mine2], 1, m, partner)
-        else:
-            from_source[m] = remote(xs.at[m, 0], xb.at[m, tp], 0, m, peer)
-            to_partner[m] = remote(xb.at[m, tp], xb.at[m, tp], 1, m, partner)
-            to_across[m] = remote(xb.at[m, tp], xb.at[m, tp], 2, m, across)
-            relay[m] = remote(xb.at[m, over_tp], xb.at[m, over_tp], 3, m, partner)
-    hid_partner, hid_across, hid_relay, back = [], [], [], [None] * n_ep
-    for m in range(n_ep):
-        hid_partner.append(remote(hb.at[m, tp], hb.at[m, tp], 4, m, partner))
-        hid_across.append(remote(hb.at[m, tp], hb.at[m, tp], 5, m, across))
-        hid_relay.append(remote(hb.at[m, over_tp], hb.at[m, over_tp], 6, m, partner))
-        if m:
-            back[m] = remote(rs.at[m], ret.at[m], 7, m, {"ep": flip(ep, m, n_ep)})
-
-    for m in send_order(n_ep):
-        chosen = place[m].astype(BF16)
+
+    def near_rows(m):
+        return remote(xs.at[m], xb.at[m, mine2], 0, m, source_of(m))
+
+    def near_partner(m):
+        return remote(xb.at[m, mine2], xb.at[m, mine2], 1, m, partner)
+
+    def far_rows(m):
+        return remote(xs.at[m, 0], xb.at[m, tp], 0, m, source_of(m))
+
+    def far_rows_over(m):
+        return remote(xs.at[m, 1], xb.at[m, over_tp], 12, m, source_of(m))
+
+    def far_partner(m):
+        return remote(xb.at[m, tp], xb.at[m, tp], 1, m, partner)
+
+    def far_across(m):
+        return remote(xb.at[m, tp], xb.at[m, tp], 2, m, across)
+
+    def far_relay(m):
+        return remote(xb.at[m, over_tp], xb.at[m, over_tp], 3, m, partner)
+
+    mid = (tiles + 1) // 2
+    pieces = [(0, mid), (mid, tiles)]
+
+    final = turns(n_ep)[-1]
+    half_cap = cap // 2
+
+    def final_turn(m):
+        return isinstance(m, int) and m == final
+
+    def hidden_piece(m, where, p):
+        if final_turn(m):
+            return hb.at[m, where, pl.ds(p * half_cap, half_cap)]
+        lo, hi = pieces[p]
+        return hb.at[m, where, :, pl.ds(lo * tile, (hi - lo) * tile)]
+
+    def hid_partner(m, p):
+        return remote(hidden_piece(m, tp, p), hidden_piece(m, tp, p), 4 + 5 * p, m, partner)
+
+    def hid_across(m, p):
+        return remote(hidden_piece(m, tp, p), hidden_piece(m, tp, p), 5 + 5 * p, m, across)
+
+    def hid_relay(m, p):
+        return remote(hidden_piece(m, over_tp, p), hidden_piece(m, over_tp, p), 6 + 5 * p, m, partner)
+
+    def back(m):
+        return remote(rs.at[m], ret.at[m], 7, m, source_of(m))
+
+    def back_final(p):
+        at = pl.ds(p * half_cap, half_cap)
+        return remote(rs.at[final, at], ret.at[final, at], 7 + 6 * p, final, source_of(final))
+
+    def dispatch(m):
+        chosen = place(m).astype(BF16)
         if m < half:
             for k in range(2):
                 at = pl.ds(pl.multiple_of((core * 2 + k) * span, span), span)
@@ -220,16 +343,26 @@
         else:
             at = pl.ds(pl.multiple_of(tp * span, span), span)
             xs[m, 0] = matmul(chosen, nb[:, at]).astype(BF16)
-        if m == send_order(n_ep)[0]:
+            if m % quarter + half + quarter in doubled(n_ep):
+                at = pl.ds(pl.multiple_of(over_tp * span, span), span)
+                xs[m, 1] = matmul(chosen, nb[:, at]).astype(BF16)
+        if m == 1:
             pl.semaphore_wait(barrier, len(peers))
-        from_source[m].start()
-    chosen = place[0].astype(BF16)
-    for k in range(depth // span):
-        xb[0, k] = matmul(chosen, nb[:, k * span : (k + 1) * span]).astype(BF16)
-
-    def expand(m):
+        if m < half:
+            near_rows(m).start()
+        else:
+            far_rows(m).start()
+            if m % quarter + half + quarter in doubled(n_ep):
+
+                @pl.when(inner == 1)
+                def _():
+                    far_rows_over(m).start()
+
+    def expand(turn):
+        m = label(turn)
+
         def body(j, carry):
-            if m == 0:
+            if turn == 0:
                 pltpu.make_async_copy(
                     gate_hbm.at[0, :, pl.ds(0, tile)], wgu.at[j, :, pl.ds(0, tile)], w_sem.at[2 * j]
                 ).wait()
@@ -246,48 +379,87 @@
             hb[m, tp, :, pl.ds(pl.multiple_of(j * tile, tile), tile)] = hidden.astype(BF16)
             return carry
 
-        lax.fori_loop(0, tiles, body, 0)
-        hid_across[m].start()
-        hid_partner[m].start()
+        for p, (lo, hi) in enumerate(pieces):
+            lax.fori_loop(lo, hi, body, 0)
+            if not final_turn(m):
+                hid_across(m, p).start()
+                hid_partner(m, p).start()
+        if final_turn(m):
+            for p in range(2):
+                hid_across(m, p).start()
+                hid_partner(m, p).start()
 
     block = 256
 
-    def contract(m):
-        hid_partner[m].wait_recv()
-        hid_relay[m].wait_recv()
+    def contract(turn):
+        m = label(turn)
+        for p in range(len(pieces)):
+            hid_partner(m, p).wait_recv()
+            hid_relay(m, p).wait_recv()
         for n in range(out_cols // block):
             cols = slice(n * block, (n + 1) * block)
             acc = matmul(hb[m, 0], wd[0:part, cols])
             for k in range(1, hb.shape[1]):
                 acc = acc + matmul(hb[m, k], wd[k * part : (k + 1) * part, cols])
-            if m == 0:
+            if turn == 0:
                 ret[0, :, cols] = acc.astype(BF16)
             else:
                 rs[m, :, cols] = acc.astype(BF16)
-        if m:
-            back[m].start()
-
-    def pass_hidden(m):
-        hid_across[m].wait_recv()
-        hid_relay[m].start()
+        if turn:
+            back(m).start()
+
+    def last(p):
+        if p == 0:
+            hid_across(final, 0).wait_recv()
+            hid_relay(final, 0).start()
+        hid_partner(final, p).wait_recv()
+        hid_relay(final, p).wait_recv()
+        at = slice(p * half_cap, (p + 1) * half_cap)
+        for n in range(out_cols // block):
+            cols = slice(n * block, (n + 1) * block)
+            acc = matmul(hb[final, 0, at], wd[0:part, cols])
+            for k in range(1, hb.shape[1]):
+                acc = acc + matmul(hb[final, k, at], wd[k * part : (k + 1) * part, cols])
+            rs[final, at, cols] = acc.astype(BF16)
+        back_final(p).start()
+        if p == 0:
+            hid_across(final, 1).wait_recv()
+            hid_relay(final, 1).start()
+
+    def pass_hidden(turn):
+        for p in range(len(pieces)):
+            hid_across(label(turn), p).wait_recv()
+            hid_relay(label(turn), p).start()
 
     def pass_near(m):
-        from_source[m].wait_recv()
-        to_partner[m].start()
-
-    def pass_far(m):
-        from_source[m].wait_recv()
-        to_across[m].start()
-        to_partner[m].start()
-
-    def pass_relay(m):
-        to_across[m].wait_recv()
-        relay[m].start()
-
-    def ready(m):
-        to_partner[m].wait_recv()
-        if m >= half:
-            relay[m].wait_recv()
+        near_rows(m).wait_recv()
+        near_partner(m).start()
+
+    def pass_both(turn):
+        m = label(turn)
+        far_rows(m).wait_recv()
+        far_partner(m).start()
+        far_rows_over(m).wait_recv()
+        far_relay(m).start()
+
+    def pass_far(turn):
+        m = label(turn)
+        far_rows(m).wait_recv()
+        far_across(m).start()
+        far_partner(m).start()
+
+    def pass_relay(turn):
+        m = label(turn)
+        far_across(m).wait_recv()
+        far_relay(m).start()
+
+    def ready(turn):
+        m = label(turn)
+        if turn < half:
+            near_partner(m).wait_recv()
+        else:
+            far_partner(m).wait_recv()
+            far_relay(m).wait_recv()
 
     mix_rows, channels = outer.shape
     halo = padded.shape[0] - mix_rows
@@ -298,25 +470,32 @@
     mix_relay = remote(grouped.at[over_tp], grouped.at[over_tp], 8, 3, partner)
 
     def mix_project():
-        normalize(mix_ref, mix_gain_ref, na)
+        for copy in fetch_small[3:]:
+            copy.wait()
+        normalize(mix_ref, mix_gain_ref, na, 0, mix_rows)
         for copy in fetch_mix:
             copy.wait()
         outer[...] = matmul(na[...], wmix[0]).astype(BF16)
         inner = matmul(na[...], wmix[1]).astype(BF16).astype(F32)
         padded[pl.ds(halo, mix_rows), :] = inner * matmul(na[...], wmix[2]).astype(BF16).astype(F32)
-        send_halo.start()
-
-    def mix_convolve():
-        send_halo.wait_recv()
+
+        @pl.when(ep < n_ep - 1)
+        def _():
+            send_halo.start()
+
+        @pl.when(ep == 0)
+        def _():
+            padded[pl.ds(0, halo), :] = jnp.zeros((halo, channels), F32)
+
+    def mix_convolve(_):
+        @pl.when(ep > 0)
+        def _():
+            send_halo.wait_recv()
+
         taps = kernel_ref[...].astype(F32)
-        row = lax.broadcasted_iota(jnp.int32, (mix_rows, channels), 0)
-        row = row + jnp.where(ep == 0, 0, mix_rows)
         conv = taps[2:3, :] * padded[pl.ds(halo, mix_rows), :]
         for back_by in (1, 2):
-            shifted = padded[pl.ds(halo - back_by, mix_rows), :]
-            conv = conv + taps[2 - back_by : 3 - back_by, :] * jnp.where(
-                row >= back_by, shifted, 0.0
-            )
+            conv = conv + taps[2 - back_by : 3 - back_by, :] * padded[pl.ds(halo - back_by, mix_rows), :]
         gated = outer[...].astype(F32) * conv
         squares = gated * gated
         group = lax.broadcasted_iota(jnp.int32, (mix_rows, channels), 1) // GROUP
@@ -328,7 +507,7 @@
         mix_across.start()
         mix_partner.start()
 
-    def mix_pass():
+    def mix_pass(_):
         mix_across.wait_recv()
         mix_relay.start()
 
@@ -342,62 +521,84 @@
         mix_o_ref[...] = acc.astype(BF16)
 
     def build_weights():
+        fetch_small[2].wait()
         for m in range(n_ep):
             picked = jnp.where(first == flip(ep, m, n_ep), weight_ref[0:1, :], weight_ref[1:2, :])
-            scaled = (place[m] * picked).T
+            scaled = (place(m) * picked).T
             high = scaled.astype(BF16)
             whi[:, m * cap : (m + 1) * cap] = high
             wlo[:, m * cap : (m + 1) * cap] = (scaled - high.astype(F32)).astype(BF16)
 
-    def near(m):
-        pass_near(m)
-        ready(m)
-        expand(m)
-
-    def far(m):
-        pass_relay(m)
-        ready(m)
-        expand(m)
-
-    def finish(m):
-        pass_hidden(m)
-        contract(m)
-
-    steps = dict(
-        near=near, far=far, finish=finish, pass_far=pass_far, pass_hidden=pass_hidden,
-        contract=contract,
-    )
+    def gather(turn):
+        m = label(turn)
+        if turn == final:
+            back_final(0).wait_recv()
+            back_final(1).wait_recv()
+        elif turn:
+            back(m).wait_recv()
+        else:
+            mix_contract()
+        cols = pl.ds(m * cap if turn < half else pl.multiple_of(m * cap, cap), cap)
+        high = matmul(whi[:, cols], ret[m])
+        low = matmul(wlo[:, cols], ret[m])
+        if turn == 0:
+            total[...] = high + low
+        else:
+            total[...] += high + low
+
+    first_sends, later_sends, last_sends = send_order(n_ep)
+    for m in first_sends:
+        dispatch(m)
+    chosen = place(0).astype(BF16)
+    for k in range(depth // span):
+        xb[0, k] = matmul(chosen, nb[:, k * span : (k + 1) * span]).astype(BF16)
     expand(0)
+    for m in later_sends:
+        dispatch(m)
     mix_project()
     build_weights()
-    near(1)
-    mix_convolve()
+    for m in last_sends:
+        dispatch(m)
     fetch_down.wait()
+    actions = dict(
+        last=last, near=pass_near, both=pass_both, pass_far=pass_far, far=pass_relay, ready=ready, expand=expand,
+        hidden=pass_hidden, contract=contract, mix_convolve=mix_convolve, mix=mix_pass,
+        gather=gather,
+    )
     for step, m in schedule(n_ep):
-        if step == "mix":
-            mix_pass()
-            mix_contract()
-        else:
-            steps[step](m)
-
-    total = None
-    for m in range(n_ep):
-        if m:
-            back[m].wait_recv()
-        high = matmul(whi[:, m * cap : (m + 1) * cap], ret[m])
-        low = matmul(wlo[:, m * cap : (m + 1) * cap], ret[m])
-        total = high + low if total is None else total + (high + low)
-    o_ref[...] = total.astype(BF16)
-
-    for copy in (send_halo, mix_partner, mix_across, mix_relay):
+        actions[step](m)
+    o_ref[...] = total[...].astype(BF16)
+
+    @pl.when(ep < n_ep - 1)
+    def _():
+        send_halo.wait_send()
+
+    for copy in (mix_partner, mix_across, mix_relay):
         copy.wait_send()
-    for m in range(n_ep):
-        for copy in (hid_partner[m], hid_across[m], hid_relay[m], from_source[m], back[m]):
-            if copy is not None:
+    for turn in range(n_ep):
+        m = label(turn)
+        for p in range(len(pieces)):
+            for copy in (hid_partner(m, p), hid_across(m, p), hid_relay(m, p)):
                 copy.wait_send()
-        for table in (to_partner, to_across, relay):
-            if m in table:
-                table[m].wait_send()
+        if turn == final:
+            back_final(0).wait_send()
+            back_final(1).wait_send()
+        elif turn:
+            back(m).wait_send()
+        if 0 < turn < half:
+            near_rows(m).wait_send()
+            near_partner(m).wait_send()
+        if turn >= half:
+            far_rows(m).wait_send()
+            far_partner(m).wait_send()
+            far_relay(m).wait_send()
+            if turn not in doubled(n_ep):
+                far_across(m).wait_send()
+            if turn % quarter + half + quarter in doubled(n_ep):
+
+                @pl.when(inner == 1)
+                def _():
+                    far_rows_over(m).wait_send()
 
 
 def fused(
@@ -430,40 +631,7 @@
     mix_cols = mixer_out_weight.shape[1]
     vmem = pl.BlockSpec(memory_space=pltpu.VMEM)
     hbm = pl.BlockSpec(memory_space=pl.ANY)
-    return pl.pallas_call(
-        functools.partial(experts_kernel, n_ep),
-        out_shape=(
-            jax.ShapeDtypeStruct((mix_rows, mix_cols), BF16),
-            jax.ShapeDtypeStruct((rows, out_cols), BF16),
-        ),
-        in_specs=[vmem] * 8 + [hbm] * 7,
-        out_specs=(vmem, vmem),
-        scratch_shapes=[
-            pltpu.VMEM((rows, width), BF16),
-            pltpu.VMEM((n_ep, 2, cap, span), BF16),
-            pltpu.VMEM((n_ep, n_tp, cap, span), BF16),
-            pltpu.VMEM((tiles, width, 2 * tile), BF16),
-            pltpu.VMEM((full, out_cols), BF16),
-            pltpu.VMEM((n_ep, n_tp, cap, part), BF16),
-            pltpu.VMEM((n_ep, cap, out_cols), BF16),
-            pltpu.VMEM((n_ep, cap, out_cols), BF16),
-            pltpu.VMEM((rows, n_ep * cap), BF16),
-            pltpu.VMEM((rows, n_ep * cap), BF16),
-            pltpu.VMEM((mix_rows, width), BF16),
-            pltpu.VMEM((3, width, channels), BF16),
-            pltpu.VMEM((channels * n_tp, mix_cols), BF16),
-            pltpu.VMEM((8 + mix_rows, channels), F32),
-            pltpu.VMEM((mix_rows, channels), BF16),
-            pltpu.VMEM((n_tp, mix_rows, channels), BF16),
-            pltpu.SemaphoreType.DMA((2 * tiles + 5,)),
-            pltpu.SemaphoreType.DMA((9, n_ep)),
-            pltpu.SemaphoreType.DMA((9, n_ep)),
-        ],
-        compiler_params=pltpu.CompilerParams(
-            collective_id=0, has_side_effects=True, vmem_limit_bytes=60 * 1024 * 1024
-        ),
-        name="layer",
-    )(
+    operands = (
         mixer_input,
         mixer_gain.reshape(1, -1),
         conv_kernel,
@@ -480,16 +648,54 @@
         expert_up,
         expert_down,
     )
+    return pl.pallas_call(
+        functools.partial(experts_kernel, n_ep),
+        out_shape=(
+            pltpu.VMEM((mix_rows, mix_cols), BF16),
+            pltpu.VMEM((rows, out_cols), BF16),
+        ),
+        in_specs=[hbm] * len(operands),
+        out_specs=(vmem, vmem),
+        scratch_shapes=[
+            *(pltpu.VMEM(v.shape, v.dtype) for v in operands[:8]),
+            pltpu.VMEM((rows, width), BF16),
+            pltpu.VMEM((n_ep, 2, cap, span), BF16),
+            pltpu.VMEM((n_ep, n_tp, cap, span), BF16),
+            pltpu.VMEM((tiles, width, 2 * tile), BF16),
+            pltpu.VMEM((full, out_cols), BF16),
+            pltpu.VMEM((n_ep, n_tp, cap, part), BF16),
+            pltpu.VMEM((n_ep, cap, out_cols), BF16),
+            pltpu.VMEM((n_ep, cap, out_cols), BF16),
+            pltpu.VMEM((rows, n_ep * cap), BF16),
+            pltpu.VMEM((rows, n_ep * cap), BF16),
+            pltpu.VMEM((rows, out_cols), F32),
+            pltpu.VMEM((mix_rows, width), BF16),
+            pltpu.VMEM((3, width, channels), BF16),
+            pltpu.VMEM((channels * n_tp, mix_cols), BF16),
+            pltpu.VMEM((8 + mix_rows, channels), F32),
+            pltpu.VMEM((mix_rows, channels), BF16),
+            pltpu.VMEM((n_tp, mix_rows, channels), BF16),
+            pltpu.SemaphoreType.DMA((rows // 64 + 7,)),
+            pltpu.SemaphoreType.DMA((2 * tiles + 5,)),
+            pltpu.SemaphoreType.DMA((14, n_ep)),
+            pltpu.SemaphoreType.DMA((14, n_ep)),
+        ],
+        compiler_params=pltpu.CompilerParams(
+            collective_id=0, has_side_effects=True, vmem_limit_bytes=60 * 1024 * 1024
+        ),
+        name="layer",
+    )(*operands)
 
 
 def fits(n_ep, n_tp, routes, expert_gate):
     return (
         n_tp == 4
-        and n_ep >= 4
+        and n_ep >= 8
         and n_ep & (n_ep - 1) == 0
         and routes.shape[1] == 2
         and expert_gate.shape[0] == 1
         and expert_gate.shape[2] % 128 == 0
+        and routes.shape[0] % 64 == 0
     )
 
 

time: 94.6 us -> 69.8 us (0.74); the launches traced: 93.3 us -> 69.7 us
  Pallas kernels: 89.4 us -> 67.7 us
  local copies, waits for them, and re-layouts: 3.24 us -> 1.36 us
    pallas_call x1, Pallas kernels: 89.4 us -> 67.7 us  [fused(): pl.pallas_call(functools.partial(experts_kernel, n_ep), out_shape=(pltpu....]
    unnamed x2, local copies, waits for them, and re-layouts: 3.24 us -> 1.36 us
where the time goes in v1:
time: 69.8 us; the launch traced here: 69.7 us
  Pallas kernels  67.7 us (97%)
  local copies, waits for them, and re-layouts  1.36 us (2%)
    pallas_call x1, Pallas kernels, fused(): pl.pallas_call(functools.partial(experts_kernel, n_ep), out_shape=(pltpu....  67.7 us

profile of v1, /device:TPU:11, one launch (start us, length us, event | category | flops | bytes accessed | tf_op | source)
XLA Modules:
  0.0 69.7 jit_solution(13163752513281836)
XLA Ops:
  0.6 67.7 %layer.1 = (bf16[128,512]{1,0:T(8,128)(2,1)S(1)}, bf16[256,512]{1,0:T(8,128)(2,1)S(1)}) custom-call(bf16[128,2048]{1,0:T(8,128)(2,1)} %mix_hbm.1, f32[1,2048]{1,0:T(1,128)} %bitcast.5, bf16[3,256]{1,0:T(4,128)(2,1)} %kernel_hbm.1, f32[1,256]{1,0:T(1,128)} %bitcast.9, bf16[256,2048]{1,0:T(8,128)(2,1)} %x_hbm.1, f32[1,2048]{1,0:T(1,128)} %bitcast.6, ...), custom_call_target="tpu_custom_call" | custom-call | tf_op jit(solution)/shard_map/layer/pallas_call | solution.py:651
  68.3 0.7 copy.19
  69.0 0.7 %copy.20 = bf16[256,512]{1,0:T(8,128)(2,1)} copy(bf16[256,512]{1,0:T(8,128)(2,1)S(1)} %get-tuple-element.3) | data formatting | bytes 524288

commit v2 on v1

--- a/solution.py
+++ b/solution.py
@@ -88,14 +88,15 @@
         send("expand", m, "hidden")
         if k + 1 < n_ep and order[k + 1] not in far:
             arrive(order[k + 1])
-        if k == 5:
-            send("mix_convolve", 0, "mix")
+        if k + 1 == n_ep:
+            steps += [("mix_convolve", 0)]
         if 2 <= k < n_ep - 1:
             steps += [("contract", order[k - 2])]
         take(("hidden", order[k - 1]))
     steps += [("contract", order[-2]), ("gather", 0), ("gather", 1)]
-    steps += [("last", 0), ("last", 1)]
-    return steps + [("gather", m) for m in order[2:]]
+    steps += [("last", 0), ("last", 1), ("mix", 0)]
+    steps += [("gather", m) for m in order[2:-1]]
+    return steps + [("mix_contract", 0), ("gather", order[-1])]
 
 
 def experts_kernel(
@@ -166,8 +167,6 @@
 
     barrier = pltpu.get_barrier_semaphore()
     peers = [{"ep": flip(ep, m, n_ep)} for m in range(1, n_ep)] + [partner, across]
-    for peer in peers:
-        pl.semaphore_signal(barrier, inc=1, device_id=peer, device_id_type=pl.DeviceIdType.MESH)
 
     chunk = 64
     chunks = rows // chunk
@@ -210,11 +209,12 @@
         for i, src in enumerate((outer_hbm, inner_hbm, value_hbm))
     ]
     fetch_mix_out = pltpu.make_async_copy(mix_out_hbm, wmo, w_sem.at[2 * tiles + 4])
-    fetch_small[0].start()
     for copy in fetch_x:
         copy.start()
-    for copy in fetch_small[1:-1]:
+    for copy in fetch_small[:-1]:
         copy.start()
+    for peer in peers:
+        pl.semaphore_signal(barrier, inc=1, device_id=peer, device_id_type=pl.DeviceIdType.MESH)
     for a, b in fetches:
         a.start()
         b.start()
@@ -511,7 +511,7 @@
         mix_across.wait_recv()
         mix_relay.start()
 
-    def mix_contract():
+    def mix_contract(_):
         fetch_mix_out.wait()
         mix_partner.wait_recv()
         mix_relay.wait_recv()
@@ -536,8 +536,6 @@
             back_final(1).wait_recv()
         elif turn:
             back(m).wait_recv()
-        else:
-            mix_contract()
         cols = pl.ds(m * cap if turn < half else pl.multiple_of(m * cap, cap), cap)
         high = matmul(whi[:, cols], ret[m])
         low = matmul(wlo[:, cols], ret[m])
@@ -563,7 +561,7 @@
     actions = dict(
         last=last, near=pass_near, both=pass_both, pass_far=pass_far, far=pass_relay, ready=ready, expand=expand,
         hidden=pass_hidden, contract=contract, mix_convolve=mix_convolve, mix=mix_pass,
-        gather=gather,
+        gather=gather, mix_contract=mix_contract,
     )
     for step, m in schedule(n_ep):
         actions[step](m)

time: 69.8 us -> 69.6 us (level)
  no operation moved by 1% of the time
where the time goes in v2:
time: 69.6 us; the launch traced here: 69.4 us
  Pallas kernels  67.4 us (97%)
  local copies, waits for them, and re-layouts  1.36 us (2%)
    pallas_call x1, Pallas kernels, fused(): pl.pallas_call(functools.partial(experts_kernel, n_ep), out_shape=(pltpu....  67.4 us

profile of v2, /device:TPU:11, one launch (start us, length us, event | category | flops | bytes accessed | tf_op | source)
XLA Modules:
  0.0 69.4 jit_solution(3792962417801247162)
XLA Ops:
  0.6 67.4 %layer.1 = (bf16[128,512]{1,0:T(8,128)(2,1)S(1)}, bf16[256,512]{1,0:T(8,128)(2,1)S(1)}) custom-call(bf16[128,2048]{1,0:T(8,128)(2,1)} %mix_hbm.1, f32[1,2048]{1,0:T(1,128)} %bitcast.5, bf16[3,256]{1,0:T(4,128)(2,1)} %kernel_hbm.1, f32[1,256]{1,0:T(1,128)} %bitcast.9, bf16[256,2048]{1,0:T(8,128)(2,1)} %x_hbm.1, f32[1,2048]{1,0:T(1,128)} %bitcast.6, ...), custom_call_target="tpu_custom_call" | custom-call | tf_op jit(solution)/shard_map/layer/pallas_call | solution.py:649
  68.1 0.7 copy.19
  68.7 0.7 %copy.20 = bf16[256,512]{1,0:T(8,128)(2,1)} copy(bf16[256,512]{1,0:T(8,128)(2,1)S(1)} %get-tuple-element.3) | data formatting | bytes 524288
